TPU v7x, 32 devices: a whole 2x2x4 slice. The times are simulated.
32 devices in a mesh: ep: 4 (over y, x), tp: 8 (over z, core).
Axes of the slice: x: 2, y: 2, z: 4, core: 2. Of those that a mesh axis runs over, the one named last changes fastest.
Arguments:
- queries: bfloat16 [4096, 1024], P('ep', 'tp'), may hold values from -6 to 6
- keys: bfloat16 [4096, 256], P('ep'), may hold values from -6 to 6, as said below
- values: bfloat16 [4096, 256], P('ep'), may hold values from -6 to 6
- slopes: float32 [16], P('tp'), may hold values from 0.002 to 0.08
- sinks: float32 [16], P('tp'), may hold values from 2 to 6
- out_weight: bfloat16 [1024, 2048], P('tp'), may hold values from -0.1875 to 0.1875
- mix_gain: float32 [2048], replicated, may hold values from 0.1 to 1.9
- moe_input: bfloat16 [4096, 2048], P(('ep', 'tp')), may hold values from -6 to 6
- in_gain: float32 [2048], replicated, may hold values from 0.1 to 1.9
- out_gain: float32 [2048], replicated, may hold values from 0.1 to 1.9
- group_router: bfloat16 [2048, 4], replicated, may hold values from -0.125 to 0.125
- expert_router: bfloat16 [2048, 4], replicated, may hold values from -0.125 to 0.125
- routes: int32 [4096, 2], P(('ep', 'tp')), may hold values from 0 to 3, all different within a row; in each aligned block of 128 rows (0 to 127, 128 to 255, ...) at most 96 rows name the same one
- gate_weight: bfloat16 [4, 2048, 1024], P('ep', None, 'tp'), may hold values from -0.125 to 0.125
- up_weight: bfloat16 [4, 2048, 1024], P('ep', None, 'tp'), may hold values from -0.125 to 0.125
- down_weight: bfloat16 [4, 2048, 1024], P('ep', None, 'tp'), may hold values from -0.1875 to 0.1875
Outputs:
- mixer_output: bfloat16 [4096, 2048], P(('ep', 'tp'))
- moe_output: bfloat16 [4096, 2048], P(('ep', 'tp'))
Inputs may be any that keep to these rules, and one draw needn't show every extreme that they name: `keys`: keys share one value range with the queries. `routes`: A token names 2 different experts. Among the rows of one device no expert is named more than 96 times, a bound that some block reaches in every draw.
All inputs are finite; a program needn't handle non-finite values.
Results may differ from a plain program's by a relative error of at most 0.018.
Values may be sent and summed in bfloat16 or wider, within the bound.
No kernel may reach another device: no remote copies, remote signals or barrier semaphores. Data moves between devices by JAX's collectives and lax.ppermute only.
A program may use at most 128 MiB of HBM per device.

v0:
```python
import math
import jax
import jax.numpy as jnp
from jax import lax
from jax.sharding import PartitionSpec as P

HEADS = 16
HD = 64
KV_HEADS = 4
WINDOW = 128
eps = 1e-06


def shifted(block, axis, distance):
    devices = range(lax.axis_size(axis))
    route = [(i - distance, i) for i in devices if i - distance in devices]
    return lax.ppermute(block, axis, route)


def scale_rows(matrix, gain):
    mean_square = jnp.mean(matrix * matrix, axis=-1, keepdims=True)
    return matrix * lax.rsqrt(mean_square + eps) * gain


def per_device(
    queries,
    keys,
    values,
    slopes,
    sinks,
    out_weight,
    mix_gain,
    moe_input,
    in_gain,
    out_gain,
    group_router,
    expert_router,
    routes,
    gate_weight,
    up_weight,
    down_weight,
):
    rows_group = queries.shape[0]
    local_heads = slopes.shape[0]
    per_kv = HEADS // KV_HEADS
    kv_index = lax.axis_index("tp") * local_heads // per_kv
    own_keys = lax.dynamic_slice_in_dim(keys, kv_index * HD, HD, 1)
    own_values = lax.dynamic_slice_in_dim(values, kv_index * HD, HD, 1)
    rim_keys, rim_values = shifted(
        (own_keys[rows_group - WINDOW :], own_values[rows_group - WINDOW :]), "ep", 1
    )
    blocks = rows_group // WINDOW
    key_blocks = own_keys.reshape(blocks, WINDOW, HD)
    value_blocks = own_values.reshape(blocks, WINDOW, HD)
    key_span = jnp.concatenate(
        [jnp.concatenate([rim_keys[None], key_blocks[:-1]], axis=0), key_blocks], axis=1
    )
    value_span = jnp.concatenate(
        [jnp.concatenate([rim_values[None], value_blocks[:-1]], axis=0), value_blocks], axis=1
    )
    query_blocks = queries.reshape(blocks, WINDOW, local_heads, HD)
    scores = jnp.einsum(
        "nqhd,nsd->nhqs", query_blocks, key_span, preferred_element_type=jnp.float32
    ) * (1.0 / math.sqrt(HD))
    query_index = jnp.arange(WINDOW, dtype=jnp.int32)[:, None]
    key_index = jnp.arange(2 * WINDOW, dtype=jnp.int32)[None, :]
    distance = query_index + WINDOW - key_index
    key_position = (
        lax.axis_index("ep") * rows_group
        + jnp.arange(blocks, dtype=jnp.int32)[:, None, None] * WINDOW
        + key_index[None]
        - WINDOW
    )
    valid = ((distance >= 0) & (distance < WINDOW))[None] & (key_position >= 0)
    scores = scores - slopes[None, :, None, None] * distance.astype(jnp.float32)[None, None]
    scores = jnp.where(valid[:, None], scores, -jnp.inf)
    sink = sinks[None, :, None, None]
    top = jnp.maximum(jnp.max(scores, axis=-1, keepdims=True), sink)
    weights = jnp.exp(scores - top)
    denom = jnp.sum(weights, axis=-1, keepdims=True) + jnp.exp(sink - top)
    probs = (weights / denom).astype(jnp.bfloat16)
    attention = jnp.einsum("nhqs,nsd->nqhd", probs, value_span, preferred_element_type=jnp.float32)
    attention = attention.astype(jnp.bfloat16).reshape(rows_group, local_heads * HD)
    own_rows = moe_input.shape[0]
    projected = lax.psum_scatter(
        jnp.dot(attention, out_weight, preferred_element_type=jnp.float32).astype(jnp.bfloat16),
        "tp",
        scatter_dimension=0,
        tiled=True,
    ).astype(jnp.float32)
    mixer_output = scale_rows(projected, mix_gain).astype(jnp.bfloat16)
    normed = scale_rows(moe_input.astype(jnp.float32), in_gain).astype(jnp.bfloat16)
    group_logits = jnp.dot(normed, group_router, preferred_element_type=jnp.float32)
    expert_logits = jnp.dot(normed, expert_router, preferred_element_type=jnp.float32)
    experts = expert_router.shape[1]
    groups = group_router.shape[1]
    per_group = experts // groups
    visits = routes.shape[1]
    expert_match = routes[:, :, None] == jnp.arange(experts, dtype=jnp.int32)[None, None, :]
    picked_logits = jnp.sum(jnp.where(expert_match, expert_logits[:, None, :], 0.0), axis=-1)
    group_prob = jax.nn.softmax(group_logits, axis=-1)
    group_match = (routes // per_group)[:, :, None] == jnp.arange(groups, dtype=jnp.int32)[
        None, None, :
    ]
    picked_group = jnp.sum(jnp.where(group_match, group_prob[:, None, :], 0.0), axis=-1)
    route_weight = picked_group * jax.nn.softmax(picked_logits, axis=-1)
    capacity = max(2, 3 * own_rows * visits // (2 * experts))
    match_int = expert_match.astype(jnp.int32).reshape(own_rows * visits, experts)
    before = jnp.cumsum(match_int, axis=0) - match_int
    slot = jnp.sum(before * match_int, axis=-1)
    position = (routes.reshape(-1) * capacity + slot).reshape(own_rows, visits)
    slot_ids = jnp.arange(experts * capacity, dtype=jnp.int32)
    placement = jnp.any(position[None, :, :] == slot_ids[:, None, None], axis=-1).astype(
        jnp.bfloat16
    )
    outgoing = jnp.dot(placement, normed, preferred_element_type=jnp.float32).astype(jnp.bfloat16)
    local_experts = gate_weight.shape[0]
    outgoing = outgoing.reshape(lax.axis_size("ep"), local_experts, capacity, normed.shape[1])
    arrived = lax.all_to_all(outgoing, "ep", split_axis=0, concat_axis=0, tiled=True)
    gate_piece = lax.all_gather(gate_weight, "tp", axis=2, tiled=True)
    up_piece = lax.all_gather(up_weight, "tp", axis=2, tiled=True)
    down_piece = lax.all_gather(down_weight, "tp", axis=2, tiled=True)
    gate = jnp.einsum("sxcd,xdf->sxcf", arrived, gate_piece, preferred_element_type=jnp.float32)
    up = jnp.einsum("sxcd,xdf->sxcf", arrived, up_piece, preferred_element_type=jnp.float32)
    hidden = (jax.nn.silu(gate) * up).astype(jnp.bfloat16)
    results = jnp.einsum("sxcf,xdf->sxcd", hidden, down_piece, preferred_element_type=jnp.float32)
    returned = lax.all_to_all(
        results.astype(jnp.bfloat16), "ep", split_axis=0, concat_axis=0, tiled=True
    )
    flat_back = returned.reshape(experts * capacity, returned.shape[3])
    picked_rows = jnp.take(flat_back, position.reshape(-1), axis=0).reshape(
        own_rows, visits, flat_back.shape[1]
    )
    moe = jnp.sum(route_weight[:, :, None] * picked_rows.astype(jnp.float32), axis=1)
    moe_output = scale_rows(moe, out_gain).astype(jnp.bfloat16)
    return (mixer_output, moe_output)


def solution(mesh):
    return jax.shard_map(
        per_device,
        mesh=mesh,
        in_specs=(
            P("ep", "tp"),
            P("ep", None),
            P("ep", None),
            P("tp"),
            P("tp"),
            P("tp", None),
            P(),
            P(("ep", "tp"), None),
            P(),
            P(),
            P(),
            P(),
            P(("ep", "tp"), None),
            P("ep", None, "tp"),
            P("ep", None, "tp"),
            P("ep", None, "tp"),
        ),
        out_specs=(P(("ep", "tp"), None), P(("ep", "tp"), None)),
        check_vma=False,
    )
```

profile of v0, /device:TPU:0, one launch (start us, length us, event | category | flops | bytes accessed | tf_op | source)
XLA Modules:
  0.0 222.8 jit_solution(3067624268574023449)
XLA Ops:
  7.2 0.7 all-gather.6.cloned.1.call-update
  8.0 0.7 all-gather.4.cloned.1.call-update
  8.7 0.7 all-gather.8.cloned.1.call-update
  9.5 1.2 constant_dynamic-slice_fusion
  10.9 4.9 %collective-permute-start.1 = (bf16[128,64]{0,1:T(8,128)(2,1)S(1)}, bf16[128,64]{0,1:T(8,128)(2,1)S(1)}, u32[]{:S(2)}, u32[]{:S(2)}) collective-permute-start(bf16[128,64]{0,1:T(8,128)(2,1)S(1)} %slice.36), channel_id=1, source_target_pairs={{0,8},{8,16},{16,24},{1,9},{9,17},{17,25},{2,10},{10,18},{18,26},{... | collective-permute-start | bytes 49160 | tf_op jit(solution)/shard_map/ppermute | solution.py:17
  15.9 3.4 %collective-permute-start = (bf16[128,64]{0,1:T(8,128)(2,1)S(1)}, bf16[128,64]{0,1:T(8,128)(2,1)S(1)}, u32[]{:S(2)}, u32[]{:S(2)}) collective-permute-start(bf16[128,64]{0,1:T(8,128)(2,1)S(1)} %slice.34), channel_id=1, source_target_pairs={{0,8},{8,16},{16,24},{1,9},{9,17},{17,25},{2,10},{10,18},{18,26},{... | collective-permute-start | bytes 49160 | tf_op jit(solution)/shard_map/ppermute | solution.py:17
  19.6 0.3 broadcast_and_fusion
  20.1 0.2 reshape.313
  20.3 0.6 fusion.73
  21.1 0.3 fusion.13
  21.5 0.5 fusion.20
  22.2 3.2 %convolution_convert_fusion = bf16[1024,2048]{1,0:T(8,128)(2,1)} fusion(bf16[128,2048]{1,0:T(8,128)(2,1)S(1)} %copy-done, bf16[16,8,8,128]{3,2,1,0:T(8,128)(2,1)S(1)} %bitcast.155), kind=kOutput, calls=%fused_computation.7 | convolution fusion | flops 538968064 | bytes 4980736 | tf_op jit(solution)/shard_map/dot_general | solution.py:86
  25.4 0.6 copy-done.3
  26.5 1.2 reduce-window.6
  28.6 1.8 convolution_convert_fusion.1
  30.4 3.9 %all-to-all-start = ((bf16[4,1,96,2048]{3,2,1,0:T(8,128)(2,1)}), bf16[4,1,96,2048]{3,2,1,0:T(8,128)(2,1)S(1)}, u32[]{:S(2)}, u32[]{:S(2)}) async-start(bf16[4,1,96,2048]{3,2,1,0:T(8,128)(2,1)} %bitcast.11), calls=%async_computation.1 | async-start | bytes 3145728 | tf_op jit(solution)/shard_map/all_to_all | solution.py:119
  34.3 0.3 fusion.74
  34.7 0.3 fusion.68
  35.5 17.6 %all-to-all-done = bf16[4,1,96,2048]{3,2,1,0:T(8,128)(2,1)S(1)} async-done(((bf16[4,1,96,2048]{3,2,1,0:T(8,128)(2,1)}), bf16[4,1,96,2048]{3,2,1,0:T(8,128)(2,1)S(1)}, u32[]{:S(2)}, u32[]{:S(2)}) %all-to-all-start) | async-done | bytes 1572896 | tf_op jit(solution)/shard_map/all_to_all | solution.py:119
  53.1 7.1 %all-gather.6.cloned.1.call-done = bf16[1,2048,1024]{2,1,0:T(8,128)(2,1)} async-done(((bf16[1,2048,128]{2,1,0:T(8,128)(2,1)}), bf16[1,2048,1024]{2,1,0:T(8,128)(2,1)}) %all-gather.6.cloned.1.call-update) | async-done | bytes 4194320 | tf_op jit(solution)/shard_map/all_gather | solution.py:121
  60.2 5.1 %fusion.2 = f32[4,96,1024]{2,1,0:T(8,128)} fusion(bf16[1,2048,1024]{2,1,0:T(8,128)(2,1)} %all-gather.6.cloned.1.call-done, bf16[4,1,96,2048]{3,2,1,0:T(8,128)(2,1)S(1)} %all-to-all-done), kind=kOutput, calls=%fused_computation.3 | convolution fusion | flops 1610612736 | bytes 7340032 | tf_op jit(solution)/shard_map/sxcd,xdf->sxcf/dot_general | solution.py:124
  65.3 42.5 %all-gather.4.cloned.1.call-done = bf16[1,2048,1024]{2,1,0:T(8,128)(2,1)} async-done(((bf16[1,2048,128]{2,1,0:T(8,128)(2,1)}), bf16[1,2048,1024]{2,1,0:T(8,128)(2,1)}) %all-gather.4.cloned.1.call-update) | async-done | bytes 4194320 | tf_op jit(solution)/shard_map/all_gather | solution.py:120
  107.8 47.6 %all-gather.8.cloned.1.call-done = bf16[1,2048,1024]{2,1,0:T(8,128)(2,1)} async-done(((bf16[1,2048,128]{2,1,0:T(8,128)(2,1)}), bf16[1,2048,1024]{2,1,0:T(8,128)(2,1)}) %all-gather.8.cloned.1.call-update) | async-done | bytes 4194320 | tf_op jit(solution)/shard_map/all_gather | solution.py:122
  155.4 8.6 %fusion.9 = bf16[4,1,96,2048]{3,2,1,0:T(8,128)(2,1)} fusion(bf16[1,2048,1024]{2,1,0:T(8,128)(2,1)} %all-gather.8.cloned.1.call-done, f32[4,96,1024]{2,1,0:T(8,128)} %fusion.2, bf16[1,2048,1024]{2,1,0:T(8,128)(2,1)} %all-gather.4.cloned.1.call-done, bf16[4,1,96,2048]{3,2,1,0:T(8,128)(2,1)S(1)} %all-to-all-done), kind=kOutput, calls=%fused_computation.10 | convolution fusion | flops 3224371200 | bytes 13107200 | tf_op jit(solution)/shard_map/sxcf,xdf->sxcd/dot_general | solution.py:126
  164.1 3.9 %all-to-all-start.1 = ((bf16[4,1,96,2048]{3,2,1,0:T(8,128)(2,1)}), bf16[4,1,96,2048]{3,2,1,0:T(8,128)(2,1)S(1)}, u32[]{:S(2)}, u32[]{:S(2)}) async-start(bf16[4,1,96,2048]{3,2,1,0:T(8,128)(2,1)} %fusion.9), calls=%async_computation.2 | async-start | bytes 3145728 | tf_op jit(solution)/shard_map/all_to_all | solution.py:127
  168.1 37.6 %reduce-scatter.2.cloned.1.call-done = bf16[128,2048]{1,0:T(8,128)(2,1)} async-done(((bf16[1024,2048]{1,0:T(8,128)(2,1)}), bf16[128,2048]{1,0:T(8,128)(2,1)}) %reduce-scatter.2.cloned.1.call-update) | async-done | bytes 524304 | tf_op jit(solution)/shard_map/reduce_scatter | solution.py:85
  205.7 1.2 fusion.30
  207.0 2.0 fusion.32
  209.0 1.4 gather_fusion
  210.4 0.7 gather.7
  211.1 4.1 %multiply_reduce_fusion = f32[128,2048]{1,0:T(8,128)S(1)} fusion(bf16[128,2,2048]{2,1,0:T(2,128)(2,1)S(1)} %gather.7, pred[128,2]{1,0:T(8,128)(4,1)S(1)} %copy.102, f32[128,2]{1,0:T(8,128)S(1)} %copy.96), kind=kLoop, calls=%fused_computation.13 | loop fusion | flops 1835008 | bytes 2098432 | tf_op jit(solution)/shard_map/reduce_sum | solution.py:134
  215.3 1.0 multiply_convert_fusion
  (79 shorter events, 3.2 us)
Async XLA Ops:
  7.2 15.0 %copy-start = (bf16[128,2048]{1,0:T(8,128)(2,1)S(1)}, bf16[128,2048]{1,0:T(8,128)(2,1)}, u32[]{:S(2)}) copy-start(bf16[128,2048]{1,0:T(8,128)(2,1)} %param.21) | copy-start | bytes 1572868
  7.2 53.0 %all-gather.6.cloned.1.call-start = ((), (), s32[]{:S(2)}) async-start(), calls=%async_computation.5 | async-start | bytes 4718592 | tf_op jit(solution)/shard_map/all_gather | solution.py:121
  7.9 12.0 %copy-start.8 = (f32[2]{0:T(128)S(1)}, f32[2]{0:T(128)}, u32[]{:S(2)}) copy-start(f32[2]{0:T(128)} %param.19) | copy-start | bytes 28
  7.9 99.9 %all-gather.4.cloned.1.call-start = ((), (), s32[]{:S(2)}) async-start(), calls=%async_computation.4 | async-start | bytes 4718592 | tf_op jit(solution)/shard_map/all_gather | solution.py:120
  8.7 11.4 %copy-start.2 = (bf16[1024,128]{1,0:T(8,128)(2,1)S(1)}, bf16[1024,128]{1,0:T(8,128)(2,1)}, u32[]{:S(2)}) copy-start(bf16[1024,128]{1,0:T(8,128)(2,1)} %param.16) | copy-start | bytes 786436
  8.7 146.7 %all-gather.8.cloned.1.call-start = ((), (), s32[]{:S(2)}) async-start(), calls=%async_computation.6 | async-start | bytes 4718592 | tf_op jit(solution)/shard_map/all_gather | solution.py:122
  9.4 196.3 %reduce-scatter.2.cloned.1.call-start = ((), (), s32[]{:S(2)}) async-start(), calls=%async_computation.3 | async-start | bytes 4718592 | tf_op jit(solution)/shard_map/reduce_scatter | solution.py:85
  10.9 9.4 %collective-permute-start.1 = (bf16[128,64]{0,1:T(8,128)(2,1)S(1)}, bf16[128,64]{0,1:T(8,128)(2,1)S(1)}, u32[]{:S(2)}, u32[]{:S(2)}) collective-permute-start(bf16[128,64]{0,1:T(8,128)(2,1)S(1)} %slice.36), channel_id=1, source_target_pairs={{0,8},{8,16},{16,24},{1,9},{9,17},{17,25},{2,10},{10,18},{18,26},{... | collective-permute-start | bytes 49160 | tf_op jit(solution)/shard_map/ppermute | solution.py:17
  15.9 5.6 %collective-permute-start = (bf16[128,64]{0,1:T(8,128)(2,1)S(1)}, bf16[128,64]{0,1:T(8,128)(2,1)S(1)}, u32[]{:S(2)}, u32[]{:S(2)}) collective-permute-start(bf16[128,64]{0,1:T(8,128)(2,1)S(1)} %slice.34), channel_id=1, source_target_pairs={{0,8},{8,16},{16,24},{1,9},{9,17},{17,25},{2,10},{10,18},{18,26},{... | collective-permute-start | bytes 49160 | tf_op jit(solution)/shard_map/ppermute | solution.py:17
  20.3 0.7 copy-start.7
  25.4 0.7 copy-start.3
  25.4 3.0 %copy-start.1 = (bf16[128,2048]{1,0:T(8,128)(2,1)S(1)}, bf16[128,2048]{1,0:T(8,128)(2,1)}, u32[]{:S(2)}) copy-start(bf16[128,2048]{1,0:T(8,128)(2,1)} %param.23) | copy-start | bytes 1572868
  25.4 3.2 %copy-start.4 = (f32[2048]{0:T(1024)S(1)}, f32[2048]{0:T(1024)}, u32[]{:S(2)}) copy-start(f32[2048]{0:T(1024)} %param.24) | copy-start | bytes 24580
  30.4 3.9 %copy-start.9 = (bf16[2048,4]{0,1:T(4,128)(2,1)S(1)}, bf16[2048,4]{0,1:T(4,128)(2,1)}, u32[]{:S(2)}) copy-start(bf16[2048,4]{0,1:T(4,128)(2,1)} %param.26) | copy-start | bytes 49156
  30.4 4.3 %copy-start.10 = (bf16[2048,4]{0,1:T(4,128)(2,1)S(1)}, bf16[2048,4]{0,1:T(4,128)(2,1)}, u32[]{:S(2)}) copy-start(bf16[2048,4]{0,1:T(4,128)(2,1)} %param.27) | copy-start | bytes 49156
  30.4 22.6 %all-to-all-start = ((bf16[4,1,96,2048]{3,2,1,0:T(8,128)(2,1)}), bf16[4,1,96,2048]{3,2,1,0:T(8,128)(2,1)S(1)}, u32[]{:S(2)}, u32[]{:S(2)}) async-start(bf16[4,1,96,2048]{3,2,1,0:T(8,128)(2,1)} %bitcast.11), calls=%async_computation.1 | async-start | bytes 3145728 | tf_op jit(solution)/shard_map/all_to_all | solution.py:119
  164.1 42.9 %copy-start.5 = (f32[2048]{0:T(1024)S(1)}, f32[2048]{0:T(1024)}, u32[]{:S(2)}) copy-start(f32[2048]{0:T(1024)} %param.22) | copy-start | bytes 24580
  164.1 44.9 %all-to-all-start.1 = ((bf16[4,1,96,2048]{3,2,1,0:T(8,128)(2,1)}), bf16[4,1,96,2048]{3,2,1,0:T(8,128)(2,1)S(1)}, u32[]{:S(2)}, u32[]{:S(2)}) async-start(bf16[4,1,96,2048]{3,2,1,0:T(8,128)(2,1)} %fusion.9), calls=%async_computation.2 | async-start | bytes 3145728 | tf_op jit(solution)/shard_map/all_to_all | solution.py:127
  211.1 4.3 %copy-start.6 = (f32[2048]{0:T(1024)S(1)}, f32[2048]{0:T(1024)}, u32[]{:S(2)}) copy-start(f32[2048]{0:T(1024)} %param.25) | copy-start | bytes 24580
Sparse Core Ops, SparseCore 0:
  9.6 50.5 all-gather.5
  61.7 45.9 all-gather.3
  109.4 45.9 all-gather.7
  157.6 48.1 reduce-scatter.1
where the time goes:
time: 223 us
  waiting for transfers between devices  155 us (70%)
  matrix products  20.5 us (9%)
  starting transfers between devices  16.2 us (7%)
  between operations  14.2 us (6%)
  other arithmetic  11.3 us (5%)
  local copies, waits for them, and re-layouts  6.18 us (3%)
    all_gather x1, waiting for transfers between devices, per_device(): down_piece = lax.all_gather(down_weight, 'tp', axis=2, tiled=True)  47.6 us
    all_gather x1, waiting for transfers between devices, per_device(): gate_piece = lax.all_gather(gate_weight, 'tp', axis=2, tiled=True)  42.5 us
    reduce_scatter x1, waiting for transfers between devices, per_device(): lax.psum_scatter(jnp.dot(attention, out_weight, preferred_element_type=jn...  37.6 us
    all_to_all x1, waiting for transfers between devices, per_device(): lax.all_to_all(outgoing, 'ep', split_axis=0, concat_axis=0, tiled=True)  17.6 us
    dot_general x1, matrix products, per_device(): jnp.einsum('sxcf,xdf->sxcd', hidden, down_piece, preferred_element_type=j...  8.63 us
    ppermute x2, starting transfers between devices, shifted(): return lax.ppermute(block, axis, route)  8.27 us
    all_gather x1, waiting for transfers between devices, per_device(): up_piece = lax.all_gather(up_weight, 'tp', axis=2, tiled=True)  7.09 us
    dot_general x1, matrix products, per_device(): jnp.einsum('sxcd,xdf->sxcf', arrived, up_piece, preferred_element_type=jn...  5.13 us
  transfers between devices with their start and end apart: 8, of which 5 were waited for; matrix products, arithmetic and copies ran while one was open for 13% of the time, Pallas kernels for 0%

commit v1 on v0

--- a/solution.py
+++ b/solution.py
@@ -9,6 +9,18 @@
 KV_HEADS = 4
 WINDOW = 128
 eps = 1e-06
+
+
+def summed_around(array, axis, dim, product):
+    devices, index, rows = (lax.axis_size(axis), lax.axis_index(axis), array.shape[dim])
+    right = [(i, (i + 1) % devices) for i in range(devices)]
+    block, total = (array, None)
+    for turn in range(devices):
+        following = lax.ppermute(block, axis, right) if turn < devices - 1 else None
+        take_in = product(block, (index - turn) % devices * rows)
+        total = take_in if total is None else total + take_in
+        block = following
+    return total
 
 
 def shifted(block, axis, distance):
@@ -119,11 +131,20 @@
     arrived = lax.all_to_all(outgoing, "ep", split_axis=0, concat_axis=0, tiled=True)
     gate_piece = lax.all_gather(gate_weight, "tp", axis=2, tiled=True)
     up_piece = lax.all_gather(up_weight, "tp", axis=2, tiled=True)
-    down_piece = lax.all_gather(down_weight, "tp", axis=2, tiled=True)
     gate = jnp.einsum("sxcd,xdf->sxcf", arrived, gate_piece, preferred_element_type=jnp.float32)
     up = jnp.einsum("sxcd,xdf->sxcf", arrived, up_piece, preferred_element_type=jnp.float32)
     hidden = (jax.nn.silu(gate) * up).astype(jnp.bfloat16)
-    results = jnp.einsum("sxcf,xdf->sxcd", hidden, down_piece, preferred_element_type=jnp.float32)
+    results = summed_around(
+        down_weight,
+        "tp",
+        2,
+        lambda own_block, offset: jnp.einsum(
+            "sxcf,xdf->sxcd",
+            lax.dynamic_slice_in_dim(hidden, offset, own_block.shape[2], axis=3),
+            own_block,
+            preferred_element_type=jnp.float32,
+        ),
+    )
     returned = lax.all_to_all(
         results.astype(jnp.bfloat16), "ep", split_axis=0, concat_axis=0, tiled=True
     )

time: 223 us -> 203 us (0.910)
  waiting for transfers between devices: 155 us -> 126 us
  matrix products: 20.5 us -> 27.4 us
    ppermute x0 -> x7, waiting for transfers between devices: none -> 99.3 us  [summed_around(): following = lax.ppermute(block, axis, right) if turn < devices - 1 else None]
    all_gather x1 -> x0, waiting for transfers between devices: 47.6 us -> none  [per_device(): down_piece = lax.all_gather(down_weight, 'tp', axis=2, tiled=True)]
    all_gather x1, waiting for transfers between devices: 42.5 us -> 0.01 us  [per_device(): gate_piece = lax.all_gather(gate_weight, 'tp', axis=2, tiled=True)]
    all_to_all x1, waiting for transfers between devices: 17.6 us -> 0.01 us  [per_device(): lax.all_to_all(outgoing, 'ep', split_axis=0, concat_axis=0, tiled=True)]
    reduce_scatter x1, waiting for transfers between devices: 37.6 us -> 25.7 us  [per_device(): lax.psum_scatter(jnp.dot(attention, out_weight, preferred_element_type=jn...]
    all_gather x1, waiting for transfers between devices: 7.09 us -> 0.01 us  [per_device(): up_piece = lax.all_gather(up_weight, 'tp', axis=2, tiled=True)]
    dot_general x1 -> x9, matrix products: 8.63 us -> 15.4 us  [the longest x8 10.8 us: per_device(): jnp.einsum('sxcf,xdf->sxcd', lax.dynamic_slice_in_dim(hidden, offset, own...]
  transfers between devices with their start and end apart: 8 -> 14, of which waited for: 5 -> 7; matrix products, arithmetic and copies ran while one was open for 13% -> 18% of each run, Pallas kernels for 0% -> 0%
where the time goes in v1:
time: 203 us; the launch traced here: 202 us
  waiting for transfers between devices  126 us (62%)
  matrix products  27.4 us (13%)
  starting transfers between devices  15.8 us (8%)
  between operations  14.3 us (7%)
  other arithmetic  11.2 us (6%)
  local copies, waits for them, and re-layouts  7.02 us (3%)
    ppermute x7, waiting for transfers between devices, summed_around(): following = lax.ppermute(block, axis, right) if turn < devices - 1 else None  99.3 us
    reduce_scatter x1, waiting for transfers between devices, per_device(): lax.psum_scatter(jnp.dot(attention, out_weight, preferred_element_type=jn...  25.7 us
    dot_general x8, matrix products, per_device(): jnp.einsum('sxcf,xdf->sxcd', lax.dynamic_slice_in_dim(hidden, offset, own...  10.8 us
    ppermute x2, starting transfers between devices, shifted(): return lax.ppermute(block, axis, route)  8.27 us
    dot_general x1, matrix products, per_device(): jnp.einsum('sxcd,xdf->sxcf', arrived, up_piece, preferred_element_type=jn...  5.17 us
    dot_general x1, matrix products, per_device(): jnp.einsum('sxcd,xdf->sxcf', arrived, gate_piece, preferred_element_type=...  4.63 us
    reduce_sum x1, other arithmetic, per_device(): jnp.sum(route_weight[:, :, None] * picked_rows.astype(jnp.float32), axis=1)  4.07 us
  transfers between devices with their start and end apart: 14, of which 7 were waited for; matrix products, arithmetic and copies ran while one was open for 18% of the time, Pallas kernels for 0%

profile of v1, /device:TPU:0, one launch (start us, length us, event | category | flops | bytes accessed | tf_op | source)
XLA Modules:
  0.0 202.2 jit_solution(7399285977318363332)
XLA Ops:
  7.2 0.7 all-gather.5.cloned.1.call-update
  8.0 0.7 all-gather.3.cloned.1.call-update
  8.8 1.2 constant_dynamic-slice_fusion
  10.1 4.9 %collective-permute-start.1 = (bf16[128,64]{0,1:T(8,128)(2,1)S(1)}, bf16[128,64]{0,1:T(8,128)(2,1)S(1)}, u32[]{:S(2)}, u32[]{:S(2)}) collective-permute-start(bf16[128,64]{0,1:T(8,128)(2,1)S(1)} %slice.36), channel_id=1, source_target_pairs={{0,8},{8,16},{16,24},{1,9},{9,17},{17,25},{2,10},{10,18},{18,26},{... | collective-permute-start | bytes 49160 | tf_op jit(solution)/shard_map/ppermute | solution.py:29
  15.2 3.4 %collective-permute-start = (bf16[128,64]{0,1:T(8,128)(2,1)S(1)}, bf16[128,64]{0,1:T(8,128)(2,1)S(1)}, u32[]{:S(2)}, u32[]{:S(2)}) collective-permute-start(bf16[128,64]{0,1:T(8,128)(2,1)S(1)} %slice.34), channel_id=1, source_target_pairs={{0,8},{8,16},{16,24},{1,9},{9,17},{17,25},{2,10},{10,18},{18,26},{... | collective-permute-start | bytes 49160 | tf_op jit(solution)/shard_map/ppermute | solution.py:29
  19.6 0.6 fusion.94
  21.4 3.2 %convolution_convert_fusion = bf16[1024,2048]{1,0:T(8,128)(2,1)} fusion(bf16[128,2048]{1,0:T(8,128)(2,1)S(1)} %copy-done, bf16[16,8,8,128]{3,2,1,0:T(8,128)(2,1)S(1)} %bitcast.183), kind=kOutput, calls=%fused_computation.5 | convolution fusion | flops 538968064 | bytes 4980736 | tf_op jit(solution)/shard_map/dot_general | solution.py:98
  24.7 1.0 copy-done.2
  26.1 21.4 %collective-permute-done.2 = bf16[1,2048,128]{2,1,0:T(8,128)(2,1)S(1)} collective-permute-done((bf16[1,2048,128]{2,1,0:T(8,128)(2,1)S(1)}, bf16[1,2048,128]{2,1,0:T(8,128)(2,1)S(1)}, u32[]{:S(2)}, u32[]{:S(2)}) %collective-permute-start.2) | collective-permute-done | bytes 524320 | tf_op jit(solution)/shard_map/ppermute | solution.py:19
  47.5 1.2 reduce-window.6
  49.3 19.9 %collective-permute-done.3 = bf16[1,2048,128]{2,1,0:T(8,128)(2,1)S(1)} collective-permute-done((bf16[1,2048,128]{2,1,0:T(8,128)(2,1)S(1)}, bf16[1,2048,128]{2,1,0:T(8,128)(2,1)S(1)}, u32[]{:S(2)}, u32[]{:S(2)}) %collective-permute-start.3) | collective-permute-done | bytes 524320 | tf_op jit(solution)/shard_map/ppermute | solution.py:19
  69.4 10.3 %collective-permute-done.4 = bf16[1,2048,128]{2,1,0:T(8,128)(2,1)} collective-permute-done((bf16[1,2048,128]{2,1,0:T(8,128)(2,1)S(1)}, bf16[1,2048,128]{2,1,0:T(8,128)(2,1)}, u32[]{:S(2)}, u32[]{:S(2)}) %collective-permute-start.4) | collective-permute-done | bytes 524320 | tf_op jit(solution)/shard_map/ppermute | solution.py:19
  79.8 1.8 convolution_convert_fusion.1
  81.6 3.7 %all-to-all-start = ((bf16[4,1,96,2048]{3,2,1,0:T(8,128)(2,1)}), bf16[4,1,96,2048]{3,2,1,0:T(8,128)(2,1)S(1)}, u32[]{:S(2)}, u32[]{:S(2)}) async-start(bf16[4,1,96,2048]{3,2,1,0:T(8,128)(2,1)} %bitcast.11), calls=%async_computation.1 | async-start | bytes 3145728 | tf_op jit(solution)/shard_map/all_to_all | solution.py:131
  85.7 15.9 %collective-permute-done.5 = bf16[1,2048,128]{2,1,0:T(8,128)(2,1)} collective-permute-done((bf16[1,2048,128]{2,1,0:T(8,128)(2,1)}, bf16[1,2048,128]{2,1,0:T(8,128)(2,1)}, u32[]{:S(2)}, u32[]{:S(2)}) %collective-permute-start.5) | collective-permute-done | bytes 524320 | tf_op jit(solution)/shard_map/ppermute | solution.py:19
  101.9 21.7 %collective-permute-done.6 = bf16[1,2048,128]{2,1,0:T(8,128)(2,1)} collective-permute-done((bf16[1,2048,128]{2,1,0:T(8,128)(2,1)}, bf16[1,2048,128]{2,1,0:T(8,128)(2,1)}, u32[]{:S(2)}, u32[]{:S(2)}) %collective-permute-start.6) | collective-permute-done | bytes 524320 | tf_op jit(solution)/shard_map/ppermute | solution.py:19
  124.2 10.2 %collective-permute-done.7 = bf16[1,2048,128]{2,1,0:T(8,128)(2,1)S(1)} collective-permute-done((bf16[1,2048,128]{2,1,0:T(8,128)(2,1)}, bf16[1,2048,128]{2,1,0:T(8,128)(2,1)S(1)}, u32[]{:S(2)}, u32[]{:S(2)}) %collective-permute-start.7) | collective-permute-done | bytes 524320 | tf_op jit(solution)/shard_map/ppermute | solution.py:19
  134.3 5.2 %fusion = f32[4,96,1024]{2,1,0:T(8,128)} fusion(bf16[1,2048,1024]{2,1,0:T(8,128)(2,1)} %all-gather.5.cloned.1.call-done, bf16[4,1,96,2048]{3,2,1,0:T(8,128)(2,1)S(1)} %all-to-all-done), kind=kOutput, calls=%fused_computation.1 | convolution fusion | flops 1610612736 | bytes 7340032 | tf_op jit(solution)/shard_map/sxcd,xdf->sxcf/dot_general | solution.py:135
  139.5 4.6 %fusion.7 = bf16[4,1,96,1024]{3,2,0,1:T(8,128)(2,1)S(1)} fusion(f32[4,96,1024]{2,1,0:T(8,128)} %fusion, bf16[1,2048,1024]{2,1,0:T(8,128)(2,1)} %all-gather.3.cloned.1.call-done, bf16[4,1,96,2048]{3,2,1,0:T(8,128)(2,1)S(1)} %all-to-all-done), kind=kOutput, calls=%fused_computation.17 | convolution fusion | flops 1612972032 | bytes 8126464 | tf_op jit(solution)/shard_map/sxcd,xdf->sxcf/dot_general | solution.py:134
  145.3 1.6 fusion.27
  147.0 1.6 fusion.29
  148.6 1.7 fusion.31
  150.3 0.6 fusion.33
  151.9 3.5 %fusion.4 = bf16[4,1,96,2048]{3,2,1,0:T(8,128)(2,1)} fusion(f32[4,96,2048]{2,1,0:T(8,128)S(1)} %fusion.25, f32[4,96,2048]{2,1,0:T(8,128)S(1)} %fusion.27, f32[4,96,2048]{2,1,0:T(8,128)S(1)} %fusion.29, f32[4,96,2048]{2,1,0:T(8,128)S(1)} %fusion.31, f32[4,96,2048]{2,1,0:T(8,128)S(1)} %fusion.33, f32[4,96,2048]{2,1,0:T(8,128)S(1)} %fusion.37, ...), kind=kOutput, calls=%fused_computation.8 | convolution fusion | flops 207618048 | bytes 24215556 | tf_op jit(solution)/shard_map/sxcf,xdf->sxcd/dot_general | solution.py:141
  155.5 3.7 %all-to-all-start.1 = ((bf16[4,1,96,2048]{3,2,1,0:T(8,128)(2,1)}), bf16[4,1,96,2048]{3,2,1,0:T(8,128)(2,1)S(1)}, u32[]{:S(2)}, u32[]{:S(2)}) async-start(bf16[4,1,96,2048]{3,2,1,0:T(8,128)(2,1)} %fusion.4), calls=%async_computation.2 | async-start | bytes 3145728 | tf_op jit(solution)/shard_map/all_to_all | solution.py:148
  159.3 25.7 %reduce-scatter.2.cloned.1.call-done = bf16[128,2048]{1,0:T(8,128)(2,1)} async-done(((bf16[1024,2048]{1,0:T(8,128)(2,1)}), bf16[128,2048]{1,0:T(8,128)(2,1)}) %reduce-scatter.2.cloned.1.call-update) | async-done | bytes 524304 | tf_op jit(solution)/shard_map/reduce_scatter | solution.py:97
  185.1 1.2 fusion.18
  186.3 2.0 %fusion.20 = bf16[128,2048]{1,0:T(8,128)(2,1)} fusion(bf16[128,2048]{1,0:T(8,128)(2,1)} %reduce-scatter.2.cloned.1.call-done, f32[2048]{0:T(1024)S(1)} %copy-done.10, f32[128]{0:T(128)S(1)} %add_rsqrt_fusion.2), kind=kLoop, calls=%fused_computation.33 | loop fusion | flops 1048576 | bytes 1057280 | tf_op jit(solution)/shard_map/convert_element_type | solution.py:103
  188.4 1.4 gather_fusion
  189.7 0.7 gather.7
  190.5 4.1 %multiply_reduce_fusion = f32[128,2048]{1,0:T(8,128)S(1)} fusion(bf16[128,2,2048]{2,1,0:T(2,128)(2,1)S(1)} %gather.7, pred[128,2]{1,0:T(8,128)(4,1)S(1)} %copy.102, f32[128,2]{1,0:T(8,128)S(1)} %copy.96), kind=kLoop, calls=%fused_computation.11 | loop fusion | flops 1835008 | bytes 2098432 | tf_op jit(solution)/shard_map/reduce_sum | solution.py:155
  194.7 1.0 multiply_convert_fusion
  (108 shorter events, 7.5 us)
Async XLA Ops:
  7.2 14.3 %copy-start = (bf16[128,2048]{1,0:T(8,128)(2,1)S(1)}, bf16[128,2048]{1,0:T(8,128)(2,1)}, u32[]{:S(2)}) copy-start(bf16[128,2048]{1,0:T(8,128)(2,1)} %param.21) | copy-start | bytes 1572868
  7.2 12.0 %copy-start.13 = (f32[2]{0:T(128)S(1)}, f32[2]{0:T(128)}, u32[]{:S(2)}) copy-start(f32[2]{0:T(128)} %param.19) | copy-start | bytes 28
  7.2 127.2 %all-gather.5.cloned.1.call-start = ((), (), s32[]{:S(2)}) async-start(), calls=%async_computation.5 | async-start | bytes 4718592 | tf_op jit(solution)/shard_map/all_gather | solution.py:133
  7.9 11.4 %copy-start.7 = (bf16[1024,128]{1,0:T(8,128)(2,1)S(1)}, bf16[1024,128]{1,0:T(8,128)(2,1)}, u32[]{:S(2)}) copy-start(bf16[1024,128]{1,0:T(8,128)(2,1)} %param.16) | copy-start | bytes 786436
  7.9 131.6 %all-gather.3.cloned.1.call-start = ((), (), s32[]{:S(2)}) async-start(), calls=%async_computation.4 | async-start | bytes 4718592 | tf_op jit(solution)/shard_map/all_gather | solution.py:132
  8.7 176.4 %reduce-scatter.2.cloned.1.call-start = ((), (), s32[]{:S(2)}) async-start(), calls=%async_computation.3 | async-start | bytes 4718592 | tf_op jit(solution)/shard_map/reduce_scatter | solution.py:97
  10.1 9.4 %collective-permute-start.1 = (bf16[128,64]{0,1:T(8,128)(2,1)S(1)}, bf16[128,64]{0,1:T(8,128)(2,1)S(1)}, u32[]{:S(2)}, u32[]{:S(2)}) collective-permute-start(bf16[128,64]{0,1:T(8,128)(2,1)S(1)} %slice.36), channel_id=1, source_target_pairs={{0,8},{8,16},{16,24},{1,9},{9,17},{17,25},{2,10},{10,18},{18,26},{... | collective-permute-start | bytes 49160 | tf_op jit(solution)/shard_map/ppermute | solution.py:29
  15.2 5.6 %collective-permute-start = (bf16[128,64]{0,1:T(8,128)(2,1)S(1)}, bf16[128,64]{0,1:T(8,128)(2,1)S(1)}, u32[]{:S(2)}, u32[]{:S(2)}) collective-permute-start(bf16[128,64]{0,1:T(8,128)(2,1)S(1)} %slice.34), channel_id=1, source_target_pairs={{0,8},{8,16},{16,24},{1,9},{9,17},{17,25},{2,10},{10,18},{18,26},{... | collective-permute-start | bytes 49160 | tf_op jit(solution)/shard_map/ppermute | solution.py:29
  19.6 0.7 copy-start.12
  24.6 1.0 copy-start.2
  24.6 1.0 copy-start.8
  24.6 44.6 %copy-start.1 = (bf16[128,2048]{1,0:T(8,128)(2,1)S(1)}, bf16[128,2048]{1,0:T(8,128)(2,1)}, u32[]{:S(2)}) copy-start(bf16[128,2048]{1,0:T(8,128)(2,1)} %param.23) | copy-start | bytes 1572868
  24.7 55.1 %copy-start.9 = (f32[2048]{0:T(1024)S(1)}, f32[2048]{0:T(1024)}, u32[]{:S(2)}) copy-start(f32[2048]{0:T(1024)} %param.24) | copy-start | bytes 24580
  25.7 21.8 %collective-permute-start.2 = (bf16[1,2048,128]{2,1,0:T(8,128)(2,1)S(1)}, bf16[1,2048,128]{2,1,0:T(8,128)(2,1)S(1)}, u32[]{:S(2)}, u32[]{:S(2)}) collective-permute-start(bf16[1,2048,128]{2,1,0:T(8,128)(2,1)S(1)} %copy-done.2), channel_id=1, source_target_pairs={{0,1},{1,2},{2,3},{3,4},{4,5},{5,6},{6,7},{7,0},{8,9},{9,10},{10,1... | collective-permute-start | bytes 1572872 | tf_op jit(solution)/shard_map/ppermute | solution.py:19
  47.4 34.2 %copy-start.3 = (bf16[1,2048,128]{2,1,0:T(8,128)(2,1)}, bf16[1,2048,128]{2,1,0:T(8,128)(2,1)S(1)}, u32[]{:S(2)}) copy-start(bf16[1,2048,128]{2,1,0:T(8,128)(2,1)S(1)} %collective-permute-done.2) | copy-start | bytes 1572868
  47.5 21.8 %collective-permute-start.3 = (bf16[1,2048,128]{2,1,0:T(8,128)(2,1)S(1)}, bf16[1,2048,128]{2,1,0:T(8,128)(2,1)S(1)}, u32[]{:S(2)}, u32[]{:S(2)}) collective-permute-start(bf16[1,2048,128]{2,1,0:T(8,128)(2,1)S(1)} %collective-permute-done.2), channel_id=1, source_target_pairs={{0,1},{1,2},{2,3},{3,4},{4,5},{5,6},{6,7},{7,0},{8,9},{9,10},{10,1... | collective-permute-start | bytes 1572872 | tf_op jit(solution)/shard_map/ppermute | solution.py:19
  69.2 12.4 %copy-start.5 = (bf16[1,2048,128]{2,1,0:T(8,128)(2,1)}, bf16[1,2048,128]{2,1,0:T(8,128)(2,1)S(1)}, u32[]{:S(2)}) copy-start(bf16[1,2048,128]{2,1,0:T(8,128)(2,1)S(1)} %collective-permute-done.3) | copy-start | bytes 1572868
  69.2 10.5 %collective-permute-start.4 = (bf16[1,2048,128]{2,1,0:T(8,128)(2,1)S(1)}, bf16[1,2048,128]{2,1,0:T(8,128)(2,1)}, u32[]{:S(2)}, u32[]{:S(2)}) collective-permute-start(bf16[1,2048,128]{2,1,0:T(8,128)(2,1)S(1)} %collective-permute-done.3), channel_id=1, source_target_pairs={{0,1},{1,2},{2,3},{3,4},{4,5},{5,6},{6,7},{7,0},{8,9},{9,10},{10,1... | collective-permute-start | bytes 1572872 | tf_op jit(solution)/shard_map/ppermute | solution.py:19
  79.7 21.8 %collective-permute-start.5 = (bf16[1,2048,128]{2,1,0:T(8,128)(2,1)}, bf16[1,2048,128]{2,1,0:T(8,128)(2,1)}, u32[]{:S(2)}, u32[]{:S(2)}) collective-permute-start(bf16[1,2048,128]{2,1,0:T(8,128)(2,1)} %collective-permute-done.4), channel_id=1, source_target_pairs={{0,1},{1,2},{2,3},{3,4},{4,5},{5,6},{6,7},{7,0},{8,9},{9,10},{10,1... | collective-permute-start | bytes 1572872 | tf_op jit(solution)/shard_map/ppermute | solution.py:19
  81.6 3.7 %copy-start.14 = (bf16[2048,4]{0,1:T(4,128)(2,1)S(1)}, bf16[2048,4]{0,1:T(4,128)(2,1)}, u32[]{:S(2)}) copy-start(bf16[2048,4]{0,1:T(4,128)(2,1)} %param.26) | copy-start | bytes 49156
  81.6 20.0 %copy-start.15 = (bf16[2048,4]{0,1:T(4,128)(2,1)S(1)}, bf16[2048,4]{0,1:T(4,128)(2,1)}, u32[]{:S(2)}) copy-start(bf16[2048,4]{0,1:T(4,128)(2,1)} %param.27) | copy-start | bytes 49156
  81.6 52.7 %all-to-all-start = ((bf16[4,1,96,2048]{3,2,1,0:T(8,128)(2,1)}), bf16[4,1,96,2048]{3,2,1,0:T(8,128)(2,1)S(1)}, u32[]{:S(2)}, u32[]{:S(2)}) async-start(bf16[4,1,96,2048]{3,2,1,0:T(8,128)(2,1)} %bitcast.11), calls=%async_computation.1 | async-start | bytes 3145728 | tf_op jit(solution)/shard_map/all_to_all | solution.py:131
  101.6 22.1 %collective-permute-start.6 = (bf16[1,2048,128]{2,1,0:T(8,128)(2,1)}, bf16[1,2048,128]{2,1,0:T(8,128)(2,1)}, u32[]{:S(2)}, u32[]{:S(2)}) collective-permute-start(bf16[1,2048,128]{2,1,0:T(8,128)(2,1)} %collective-permute-done.5), channel_id=1, source_target_pairs={{0,1},{1,2},{2,3},{3,4},{4,5},{5,6},{6,7},{7,0},{8,9},{9,10},{10,1... | collective-permute-start | bytes 1572872 | tf_op jit(solution)/shard_map/ppermute | solution.py:19
  123.6 10.7 %collective-permute-start.7 = (bf16[1,2048,128]{2,1,0:T(8,128)(2,1)}, bf16[1,2048,128]{2,1,0:T(8,128)(2,1)S(1)}, u32[]{:S(2)}, u32[]{:S(2)}) collective-permute-start(bf16[1,2048,128]{2,1,0:T(8,128)(2,1)} %collective-permute-done.6), channel_id=1, source_target_pairs={{0,1},{1,2},{2,3},{3,4},{4,5},{5,6},{6,7},{7,0},{8,9},{9,10},{10,1... | collective-permute-start | bytes 1572872 | tf_op jit(solution)/shard_map/ppermute | solution.py:19
  134.3 17.6 %collective-permute-start.8 = (bf16[1,2048,128]{2,1,0:T(8,128)(2,1)S(1)}, bf16[1,2048,128]{2,1,0:T(8,128)(2,1)}, u32[]{:S(2)}, u32[]{:S(2)}) collective-permute-start(bf16[1,2048,128]{2,1,0:T(8,128)(2,1)S(1)} %collective-permute-done.7), channel_id=1, source_target_pairs={{0,1},{1,2},{2,3},{3,4},{4,5},{5,6},{6,7},{7,0},{8,9},{9,10},{10,1... | collective-permute-start | bytes 1572872 | tf_op jit(solution)/shard_map/ppermute | solution.py:19
  148.6 1.7 copy-start.6
  150.3 1.1 copy-start.4
  155.5 30.8 %copy-start.10 = (f32[2048]{0:T(1024)S(1)}, f32[2048]{0:T(1024)}, u32[]{:S(2)}) copy-start(f32[2048]{0:T(1024)} %param.22) | copy-start | bytes 24580
  155.5 32.9 %all-to-all-start.1 = ((bf16[4,1,96,2048]{3,2,1,0:T(8,128)(2,1)}), bf16[4,1,96,2048]{3,2,1,0:T(8,128)(2,1)S(1)}, u32[]{:S(2)}, u32[]{:S(2)}) async-start(bf16[4,1,96,2048]{3,2,1,0:T(8,128)(2,1)} %fusion.4), calls=%async_computation.2 | async-start | bytes 3145728 | tf_op jit(solution)/shard_map/all_to_all | solution.py:148
  190.4 4.3 %copy-start.11 = (f32[2048]{0:T(1024)S(1)}, f32[2048]{0:T(1024)}, u32[]{:S(2)}) copy-start(f32[2048]{0:T(1024)} %param.25) | copy-start | bytes 24580
Sparse Core Ops, SparseCore 0:
  9.6 61.7 all-gather.4
  73.0 57.4 all-gather.2
  132.8 52.2 reduce-scatter.1
